TPU v7x, 32 devices: a whole 2x2x4 slice. The times are simulated.
32 devices in a mesh: fs: 16 (over z, y, x), tp: 2 (over core).
Axes of the slice: x: 2, y: 2, z: 4, core: 2. Of those that a mesh axis runs over, the one named last changes fastest.
Arguments:
- tokens: bfloat16 [8192, 2048], P('fs', 'tp'), may hold values from -6 to 6
- norm_gain: bfloat16 [2048], P('tp'), may hold values from 0.099609375 to 1.8984375
- proj_u: bfloat16 [2048, 2048], P('fs', 'tp'), may hold values from -0.125 to 0.125
- proj_v: bfloat16 [2048, 2048], P('fs', 'tp'), may hold values from -0.125 to 0.125
- layer_gain: bfloat16 [2048], P('tp'), may hold values from 0.099609375 to 1.8984375
- layer_shift: bfloat16 [2048], P('tp'), may hold values from -3 to 3
- mix_weight: bfloat16 [16, 128, 128], P('tp'), may hold values from -0.5 to 0.5
- mix_bias: bfloat16 [16, 128], P('tp'), may hold values from 0.099609375 to 1.8984375
- proj_out: bfloat16 [2048, 2048], P('tp', 'fs'), may hold values from -0.1875 to 0.1875
- ffn_gain: bfloat16 [2048], P('tp'), may hold values from 0.099609375 to 1.8984375
- ffn_gate: bfloat16 [2048, 4096], P('fs', 'tp'), may hold values from -0.125 to 0.125
- ffn_value: bfloat16 [2048, 4096], P('fs', 'tp'), may hold values from -0.125 to 0.125
- conv_gate: bfloat16 [3, 4096], P(None, 'tp'), may hold values from -3 to 3
- conv_value: bfloat16 [3, 4096], P(None, 'tp'), may hold values from -3 to 3
- proj_down: bfloat16 [4096, 2048], P('tp', 'fs'), may hold values from -0.125 to 0.125
Outputs:
- result: bfloat16 [8192, 2048], P('fs', 'tp')
All inputs are finite; a program needn't handle non-finite values.
Results may differ from a plain program's by a relative error of at most 0.017.
Values may be sent and summed in bfloat16 or wider, within the bound.
A program may use at most 64 MiB of HBM per device.

v0:
```python
import jax
import jax.numpy as jnp
from jax import lax
from jax.sharding import PartitionSpec as P

GROUP_DIM = 128
BLOCK = 128
SEGMENT = 64
KERNEL = 3
SEQ_LEN = 256
EPS = 1e-06


def matmul(operand, matrix):
    return jnp.dot(operand, matrix, preferred_element_type=jnp.float32)


def local_rms(values_in, gain_row):
    values = values_in.astype(jnp.float32)
    scale_row = lax.rsqrt(jnp.mean(values * values, axis=1, keepdims=True) + EPS)
    return (values * scale_row * gain_row.astype(jnp.float32)).astype(jnp.bfloat16)


def causal_taps(values, weights):
    seq_count = values.shape[0] // SEQ_LEN
    shaped = values.reshape(seq_count, SEQ_LEN, values.shape[1])
    padded = jnp.pad(shaped, ((0, 0), (KERNEL - 1, 0), (0, 0)))
    summed = jnp.zeros(shaped.shape, jnp.float32)
    for tap_index in range(KERNEL):
        summed = summed + padded[:, tap_index : tap_index + SEQ_LEN].astype(jnp.float32) * weights[
            tap_index
        ].astype(jnp.float32)
    return summed.reshape(values.shape[0], values.shape[1])


def on_device(
    tokens,
    norm_gain,
    proj_u,
    proj_v,
    layer_gain,
    layer_shift,
    mix_weight,
    mix_bias,
    proj_out,
    ffn_gain,
    ffn_gate,
    ffn_value,
    conv_gate,
    conv_value,
    proj_down,
):
    own_width = tokens.shape[1]
    whole_tokens, whole_gain, whole_ffn_gain = (
        lax.all_gather(tokens, "tp", axis=1, tiled=True),
        lax.all_gather(norm_gain, "tp", axis=0, tiled=True),
        lax.all_gather(ffn_gain, "tp", axis=0, tiled=True),
    )
    normed = local_rms(whole_tokens, whole_gain)
    row_count = normed.shape[0]
    whole_u, whole_v = (
        lax.all_gather(proj_u, "fs", axis=0, tiled=True),
        lax.all_gather(proj_v, "fs", axis=0, tiled=True),
    )
    pre_u = matmul(normed, whole_u)
    pre_v = matmul(normed, whole_v)
    act_u = jax.nn.gelu(pre_u, approximate=False)
    act_v = jax.nn.gelu(pre_v, approximate=False)
    full_width = act_v.shape[1] * lax.axis_size("tp")
    total_sum, second = lax.psum((jnp.sum(act_v, axis=1), jnp.sum(act_v * act_v, axis=1)), "tp")
    center = total_sum / full_width
    spread = second / full_width - center * center
    mixed_in = (
        (act_v - center[:, None])
        * lax.rsqrt(spread + EPS)[:, None]
        * layer_gain.astype(jnp.float32)
        + layer_shift.astype(jnp.float32)
    ).astype(jnp.bfloat16)
    groups = mixed_in.shape[1] // GROUP_DIM
    blocks = mixed_in.reshape(row_count // BLOCK, BLOCK, groups, GROUP_DIM)
    segment = jnp.arange(BLOCK) // SEGMENT
    visible = segment[None, :] <= segment[:, None]
    masked = jnp.where(visible[None], mix_weight, jnp.zeros_like(mix_weight))
    spatial = (
        jnp.einsum("gij,njgc->nigc", masked, blocks, preferred_element_type=jnp.float32)
        + mix_bias.astype(jnp.float32).T[None, :, :, None]
    )
    gated_rows = (act_u * spatial.reshape(row_count, mixed_in.shape[1])).astype(jnp.bfloat16)
    whole_out = lax.all_gather(proj_out, "fs", axis=1, tiled=True)
    partial_value = matmul(gated_rows, whole_out)
    summed = lax.psum(partial_value.astype(jnp.bfloat16), "tp").astype(jnp.float32)
    stream_rows = (whole_tokens.astype(jnp.float32) + summed).astype(jnp.bfloat16)
    normed_two = local_rms(stream_rows, whole_ffn_gain)
    stream = lax.dynamic_slice_in_dim(stream_rows, lax.axis_index("tp") * own_width, own_width, 1)
    whole_gate, whole_value = (
        lax.all_gather(ffn_gate, "fs", axis=0, tiled=True),
        lax.all_gather(ffn_value, "fs", axis=0, tiled=True),
    )
    pre_gate = matmul(normed_two, whole_gate)
    pre_value = matmul(normed_two, whole_value)
    conv_g = causal_taps(pre_gate.astype(jnp.bfloat16), conv_gate)
    conv_v = causal_taps(pre_value.astype(jnp.bfloat16), conv_value)
    hidden = (jax.nn.silu(conv_g) * conv_v).astype(jnp.bfloat16)
    whole_down = lax.all_gather(proj_down, "fs", axis=1, tiled=True)
    partial_two = matmul(hidden, whole_down)
    return (
        stream.astype(jnp.float32)
        + lax.psum_scatter(
            partial_two.astype(jnp.bfloat16), "tp", scatter_dimension=1, tiled=True
        ).astype(jnp.float32)
    ).astype(jnp.bfloat16)


def solution(mesh):
    in_specs = (
        P("fs", "tp"),
        P("tp"),
        P("fs", "tp"),
        P("fs", "tp"),
        P("tp"),
        P("tp"),
        P("tp", None, None),
        P("tp", None),
        P("tp", "fs"),
        P("tp"),
        P("fs", "tp"),
        P("fs", "tp"),
        P(None, "tp"),
        P(None, "tp"),
        P("tp", "fs"),
    )
    out_specs = P("fs", "tp")
    return jax.shard_map(
        on_device, mesh=mesh, in_specs=in_specs, out_specs=out_specs, check_vma=False
    )
```

profile of v0, /device:TPU:0, one launch (start us, length us, event | category | flops | bytes accessed | tf_op | source)
XLA Modules:
  0.0 702.0 jit_solution(10624210363305999877)
XLA Ops:
  9.4 2.1 all_gather.28
  13.6 8.6 %all-gather.8.cloned.1.call-done = bf16[512,2048]{1,0:T(8,128)(2,1)} async-done(((bf16[512,1024]{1,0:T(8,128)(2,1)}), bf16[512,2048]{1,0:T(8,128)(2,1)}) %all-gather.8.cloned.1.call-update) | async-done | bytes 2097168 | tf_op jit(solution)/shard_map/all_gather | solution.py:55
  22.2 2.2 fusion.3
  24.4 77.3 %all-gather.12.cloned.1.call-done = bf16[2048,1024]{1,0:T(8,128)(2,1)} async-done(((bf16[128,1024]{1,0:T(8,128)(2,1)}), bf16[2048,1024]{1,0:T(8,128)(2,1)}) %all-gather.12.cloned.1.call-update) | async-done | bytes 4194320 | tf_op jit(solution)/shard_map/all_gather | solution.py:63
  101.8 9.6 %fusion.111 = (f32[512]{0:T(512)S(1)}, f32[512]{0:T(512)S(1)}, f32[512,1024]{1,0:T(8,128)}) fusion(bf16[2048,1024]{1,0:T(8,128)(2,1)} %all-gather.12.cloned.1.call-done, bf16[512,2048]{1,0:T(8,128)(2,1)S(1)} %copy-done, f32[2048]{0:T(1024)S(1)} %convert_element_type.144, f32[512]{0:T(512)S(1)} %add_rsqrt_fusion.2), kind=kOutput, calls=%fused_computation.152 | convolution fusion | flops 2186804224 | bytes 8402944 | tf_op jit(solution)/shard_map/dot_general | solution.py:15
  111.4 2.6 all-reduce.2
  114.1 2.1 fusion.32
  118.3 2.9 copy.19
  121.2 57.5 %all-gather.10.cloned.1.call-done = bf16[2048,1024]{1,0:T(8,128)(2,1)} async-done(((bf16[128,1024]{1,0:T(8,128)(2,1)}), bf16[2048,1024]{1,0:T(8,128)(2,1)}) %all-gather.10.cloned.1.call-update) | async-done | bytes 4194320 | tf_op jit(solution)/shard_map/all_gather | solution.py:62
  178.8 89.9 %all-gather.14.cloned.1.call-done = bf16[1024,2048]{1,0:T(8,128)(2,1)} async-done(((bf16[1024,128]{1,0:T(8,128)(2,1)}), bf16[1024,2048]{1,0:T(8,128)(2,1)}) %all-gather.14.cloned.1.call-update) | async-done | bytes 4194320 | tf_op jit(solution)/shard_map/all_gather | solution.py:89
  268.7 14.5 %convolution_convert_fusion = bf16[512,2048]{1,0:T(8,128)(2,1)} fusion(bf16[1024,2048]{1,0:T(8,128)(2,1)} %all-gather.14.cloned.1.call-done, f32[64,8,8,128]{3,2,1,0:T(8,128)} %bitcast.51, bf16[2048,1024]{1,0:T(8,128)(2,1)} %all-gather.10.cloned.1.call-done, bf16[512,2048]{1,0:T(8,128)(2,1)S(1)} %copy-done, f32[2048]{0:T(1024)S(1)} %convert_element_type.144, ...), kind=kOutput, calls=%fused_computation.23 | convolution fusion | flops 4334813184 | bytes 14690304 | tf_op jit(solution)/shard_map/dot_general | solution.py:15
  285.3 2.1 all_gather.32
  287.5 15.4 %all-reduce.5.cloned.1.call-done = bf16[512,2048]{1,0:T(8,128)(2,1)} async-done(((bf16[512,2048]{1,0:T(8,128)(2,1)}), bf16[512,2048]{1,0:T(8,128)(2,1)}) %all-reduce.5.cloned.1.call-update) | async-done | bytes 2097168 | tf_op jit(solution)/shard_map/psum | solution.py:91
  302.8 3.9 fusion
  306.8 112.2 %all-gather.16.cloned.1.call-done = bf16[2048,2048]{1,0:T(8,128)(2,1)} async-done(((bf16[128,2048]{1,0:T(8,128)(2,1)}), bf16[2048,2048]{1,0:T(8,128)(2,1)}) %all-gather.16.cloned.1.call-update) | async-done | bytes 8388624 | tf_op jit(solution)/shard_map/all_gather | solution.py:96
  419.0 10.0 %convolution_convert_fusion.3 = bf16[512,2048]{1,0:T(8,128)(2,1)} fusion(bf16[2048,2048]{1,0:T(8,128)(2,1)} %all-gather.16.cloned.1.call-done, bf16[512,2048]{1,0:T(8,128)(2,1)} %get-tuple-element.10, f32[2048]{0:T(1024)S(1)} %convert_element_type.155, f32[512]{0:T(512)S(1)} %add_rsqrt_fusion), kind=kOutput, calls=%fused_computation.26 | convolution fusion | flops 4300210176 | bytes 12593152 | tf_op jit(solution)/shard_map/dot_general | solution.py:15
  429.0 103.2 %all-gather.18.cloned.1.call-done = bf16[2048,2048]{1,0:T(8,128)(2,1)} async-done(((bf16[128,2048]{1,0:T(8,128)(2,1)}), bf16[2048,2048]{1,0:T(8,128)(2,1)}) %all-gather.18.cloned.1.call-update) | async-done | bytes 8388624 | tf_op jit(solution)/shard_map/all_gather | solution.py:97
  532.2 8.4 %convolution_convert_fusion.2 = bf16[512,2048]{1,0:T(8,128)(2,1)S(1)} fusion(bf16[2048,2048]{1,0:T(8,128)(2,1)} %all-gather.18.cloned.1.call-done, bf16[512,2048]{1,0:T(8,128)(2,1)S(1)} %copy-done.1, f32[2048]{0:T(1024)S(1)} %convert_element_type.155, f32[512]{0:T(512)S(1)} %add_rsqrt_fusion), kind=kOutput, calls=%fused_computation.25 | convolution fusion | flops 4300210176 | bytes 12593152 | tf_op jit(solution)/shard_map/dot_general | solution.py:15
  540.7 3.0 multiply_add_fusion
  543.7 2.6 fusion.7
  546.3 128.7 %all-gather.20.cloned.1.call-done = bf16[2048,2048]{1,0:T(8,128)(2,1)} async-done(((bf16[2048,128]{1,0:T(8,128)(2,1)}), bf16[2048,2048]{1,0:T(8,128)(2,1)}) %all-gather.20.cloned.1.call-update) | async-done | bytes 8388624 | tf_op jit(solution)/shard_map/all_gather | solution.py:104
  675.0 9.9 %convolution_convert_fusion.1 = bf16[512,2048]{1,0:T(8,128)(2,1)} fusion(bf16[512,2048]{1,0:T(8,128)(2,1)} %fusion.7, bf16[2048,2048]{1,0:T(8,128)(2,1)} %all-gather.20.cloned.1.call-done), kind=kOutput, calls=%fused_computation.24 | convolution fusion | flops 4296015872 | bytes 12582912 | tf_op jit(solution)/shard_map/dot_general | solution.py:15
  684.9 8.0 %reduce-scatter.2.cloned.1.call-done = bf16[512,1024]{1,0:T(8,128)(2,1)} async-done(((bf16[512,2048]{1,0:T(8,128)(2,1)}), bf16[512,1024]{1,0:T(8,128)(2,1)}) %reduce-scatter.2.cloned.1.call-update) | async-done | bytes 1048592 | tf_op jit(solution)/shard_map/reduce_scatter | solution.py:108
  692.9 2.6 add_convert_fusion
  (46 shorter events, 9.2 us)
Async XLA Ops:
  6.5 15.7 %all-gather.8.cloned.1.call-start = ((), (), s32[]{:S(2)}) async-start(), calls=%async_computation.1 | async-start | bytes 3145728 | tf_op jit(solution)/shard_map/all_gather | solution.py:55
  7.3 94.5 %all-gather.12.cloned.1.call-start = ((), (), s32[]{:S(2)}) async-start(), calls=%async_computation.3 | async-start | bytes 4456448 | tf_op jit(solution)/shard_map/all_gather | solution.py:63
  8.0 170.8 %all-gather.10.cloned.1.call-start = ((), (), s32[]{:S(2)}) async-start(), calls=%async_computation.2 | async-start | bytes 4456448 | tf_op jit(solution)/shard_map/all_gather | solution.py:62
  8.7 259.9 %all-gather.14.cloned.1.call-start = ((), (), s32[]{:S(2)}) async-start(), calls=%async_computation.4 | async-start | bytes 4456448 | tf_op jit(solution)/shard_map/all_gather | solution.py:89
  9.3 293.5 %all-reduce.5.cloned.1.call-start = ((), (), s32[]{:S(2)}) async-start(), calls=%async_computation.5 | async-start | bytes 4194304 | tf_op jit(solution)/shard_map/psum | solution.py:91
  22.2 79.6 %copy-start = (bf16[512,2048]{1,0:T(8,128)(2,1)S(1)}, bf16[512,2048]{1,0:T(8,128)(2,1)}, u32[]{:S(2)}) copy-start(bf16[512,2048]{1,0:T(8,128)(2,1)} %all-gather.8.cloned.1.call-done) | copy-start | bytes 6291460
  114.1 2.4 copy-start.3
  283.2 2.2 copy-start.6
  283.2 4.2 copy-start.4
  283.2 4.3 copy-start.5
  283.2 135.8 %all-gather.16.cloned.1.call-start = ((), (), s32[]{:S(2)}) async-start(), calls=%async_computation.6 | async-start | bytes 8912896 | tf_op jit(solution)/shard_map/all_gather | solution.py:96
  283.8 248.4 %all-gather.18.cloned.1.call-start = ((), (), s32[]{:S(2)}) async-start(), calls=%async_computation.7 | async-start | bytes 8912896 | tf_op jit(solution)/shard_map/all_gather | solution.py:97
  284.5 390.4 %all-gather.20.cloned.1.call-start = ((), (), s32[]{:S(2)}) async-start(), calls=%async_computation.8 | async-start | bytes 8912896 | tf_op jit(solution)/shard_map/all_gather | solution.py:104
  285.3 407.6 %reduce-scatter.2.cloned.1.call-start = ((), (), s32[]{:S(2)}) async-start(), calls=%async_computation.9 | async-start | bytes 3145728 | tf_op jit(solution)/shard_map/reduce_scatter | solution.py:108
  419.0 113.3 %copy-start.1 = (bf16[512,2048]{1,0:T(8,128)(2,1)S(1)}, bf16[512,2048]{1,0:T(8,128)(2,1)}, u32[]{:S(2)}) copy-start(bf16[512,2048]{1,0:T(8,128)(2,1)} %get-tuple-element.10) | copy-start | bytes 6291460
  532.2 8.4 %copy-start.2 = (bf16[512,2048]{1,0:T(8,128)(2,1)S(1)}, bf16[512,2048]{1,0:T(8,128)(2,1)}, u32[]{:S(2)}) copy-start(bf16[512,2048]{1,0:T(8,128)(2,1)} %convolution_convert_fusion.3) | copy-start | bytes 6291460
Sparse Core Ops, SparseCore 0:
  8.9 13.2 all-gather.7
  25.0 76.7 all-gather.11
  104.5 74.1 all-gather.9
  181.3 87.3 all-gather.13
  283.3 19.4 all-reduce.4
  305.5 113.4 all-gather.15
  421.7 110.4 all-gather.17
  534.9 139.9 all-gather.19
  685.0 7.7 reduce-scatter.1
where the time goes:
time: 702 us
  waiting for transfers between devices  605 us (86%)
  matrix products  54.3 us (8%)
  other arithmetic  18.7 us (3%)
  between operations  13.3 us (2%)
    all_gather x1, waiting for transfers between devices, on_device(): whole_down = lax.all_gather(proj_down, 'fs', axis=1, tiled=True)  129 us
    all_gather x1, waiting for transfers between devices, on_device(): lax.all_gather(ffn_gate, 'fs', axis=0, tiled=True)  112 us
    all_gather x1, waiting for transfers between devices, on_device(): lax.all_gather(ffn_value, 'fs', axis=0, tiled=True)  103 us
    all_gather x1, waiting for transfers between devices, on_device(): whole_out = lax.all_gather(proj_out, 'fs', axis=1, tiled=True)  89.9 us
    all_gather x1, waiting for transfers between devices, on_device(): lax.all_gather(proj_v, 'fs', axis=0, tiled=True)  77.3 us
    all_gather x1, waiting for transfers between devices, on_device(): lax.all_gather(proj_u, 'fs', axis=0, tiled=True)  57.5 us
    dot_general x5, matrix products, matmul(): return jnp.dot(operand, matrix, preferred_element_type=jnp.float32)  52.5 us
    psum x1, waiting for transfers between devices, on_device(): lax.psum(partial_value.astype(jnp.bfloat16), 'tp').astype(jnp.float32)  15.4 us
  transfers between devices with their start and end apart: 9, of which 9 were waited for; matrix products, arithmetic and copies ran while one was open for 7% of the time, Pallas kernels for 0%

commit v1 on v0

--- a/solution.py
+++ b/solution.py
@@ -86,7 +86,12 @@
         + mix_bias.astype(jnp.float32).T[None, :, :, None]
     )
     gated_rows = (act_u * spatial.reshape(row_count, mixed_in.shape[1])).astype(jnp.bfloat16)
-    whole_out = lax.all_gather(proj_out, "fs", axis=1, tiled=True)
+    ring = [proj_out]
+    for hop in range(15):
+        ring.append(lax.ppermute(ring[-1], "fs", [(dev, (dev + 1) % 16) for dev in range(16)]))
+    whole_out = jnp.roll(
+        jnp.concatenate(ring[::-1], axis=1), (lax.axis_index("fs") + 1) * ring[0].shape[1], axis=1
+    )
     partial_value = matmul(gated_rows, whole_out)
     summed = lax.psum(partial_value.astype(jnp.bfloat16), "tp").astype(jnp.float32)
     stream_rows = (whole_tokens.astype(jnp.float32) + summed).astype(jnp.bfloat16)

time: 702 us -> 679 us (0.967)
  waiting for transfers between devices: 605 us -> 550 us
  local copies, waits for them, and re-layouts: 3.24 us -> 31.5 us
    ppermute x0 -> x15, waiting for transfers between devices: none -> 182 us  [on_device(): lax.ppermute(ring[-1], 'fs', [(dev, (dev + 1) % 16) for dev in range(16)])]
    all_gather x1 -> x0, waiting for transfers between devices: 89.9 us -> none  [on_device(): whole_out = lax.all_gather(proj_out, 'fs', axis=1, tiled=True)]
    all_gather x1, waiting for transfers between devices: 77.3 us -> 0.01 us  [on_device(): lax.all_gather(proj_v, 'fs', axis=0, tiled=True)]
    all_gather x1, waiting for transfers between devices: 57.5 us -> 0.01 us  [on_device(): lax.all_gather(proj_u, 'fs', axis=0, tiled=True)]
    unnamed x15 -> x56, local copies, waits for them, and re-layouts: 0.29 us -> 27.8 us
    all_gather x1, waiting for transfers between devices: 8.57 us -> 0.01 us  [on_device(): lax.all_gather(tokens, 'tp', axis=1, tiled=True)]
  transfers between devices with their start and end apart: 9 -> 23, of which waited for: 9 -> 20; matrix products, arithmetic and copies ran while one was open for 7% -> 11% of each run, Pallas kernels for 0% -> 0%
where the time goes in v1:
time: 679 us; the launch traced here: 678 us
  waiting for transfers between devices  550 us (81%)
  matrix products  54.2 us (8%)
  local copies, waits for them, and re-layouts  31.5 us (5%)
  other arithmetic  18.6 us (3%)
  between operations  13.6 us (2%)
    ppermute x15, waiting for transfers between devices, on_device(): lax.ppermute(ring[-1], 'fs', [(dev, (dev + 1) % 16) for dev in range(16)])  182 us
    all_gather x1, waiting for transfers between devices, on_device(): whole_down = lax.all_gather(proj_down, 'fs', axis=1, tiled=True)  129 us
    all_gather x1, waiting for transfers between devices, on_device(): lax.all_gather(ffn_gate, 'fs', axis=0, tiled=True)  112 us
    all_gather x1, waiting for transfers between devices, on_device(): lax.all_gather(ffn_value, 'fs', axis=0, tiled=True)  103 us
    dot_general x5, matrix products, matmul(): return jnp.dot(operand, matrix, preferred_element_type=jnp.float32)  52.4 us
    unnamed x56, local copies, waits for them, and re-layouts  27.8 us
  transfers between devices with their start and end apart: 23, of which 20 were waited for; matrix products, arithmetic and copies ran while one was open for 11% of the time, Pallas kernels for 0%

profile of v1, /device:TPU:0, one launch (start us, length us, event | category | flops | bytes accessed | tf_op | source)
XLA Modules:
  0.0 678.3 jit_solution(11970547701244843502)
XLA Ops:
  11.1 10.5 %collective-permute-done = bf16[1024,128]{1,0:T(8,128)(2,1)S(1)} collective-permute-done((bf16[1024,128]{1,0:T(8,128)(2,1)}, bf16[1024,128]{1,0:T(8,128)(2,1)S(1)}, u32[]{:S(2)}, u32[]{:S(2)}) %collective-permute-start) | collective-permute-done | bytes 262176 | tf_op jit(solution)/shard_map/ppermute | solution.py:91
  21.6 11.1 %collective-permute-done.1 = bf16[1024,128]{1,0:T(8,128)(2,1)S(1)} collective-permute-done((bf16[1024,128]{1,0:T(8,128)(2,1)S(1)}, bf16[1024,128]{1,0:T(8,128)(2,1)S(1)}, u32[]{:S(2)}, u32[]{:S(2)}) %collective-permute-start.1) | collective-permute-done | bytes 262176 | tf_op jit(solution)/shard_map/ppermute | solution.py:91
  32.7 13.3 %collective-permute-done.2 = bf16[1024,128]{1,0:T(8,128)(2,1)S(1)} collective-permute-done((bf16[1024,128]{1,0:T(8,128)(2,1)S(1)}, bf16[1024,128]{1,0:T(8,128)(2,1)S(1)}, u32[]{:S(2)}, u32[]{:S(2)}) %collective-permute-start.2) | collective-permute-done | bytes 262176 | tf_op jit(solution)/shard_map/ppermute | solution.py:91
  46.0 10.0 %collective-permute-done.3 = bf16[1024,128]{1,0:T(8,128)(2,1)S(1)} collective-permute-done((bf16[1024,128]{1,0:T(8,128)(2,1)S(1)}, bf16[1024,128]{1,0:T(8,128)(2,1)S(1)}, u32[]{:S(2)}, u32[]{:S(2)}) %collective-permute-start.3) | collective-permute-done | bytes 262176 | tf_op jit(solution)/shard_map/ppermute | solution.py:91
  55.9 16.0 %collective-permute-done.4 = bf16[1024,128]{1,0:T(8,128)(2,1)S(1)} collective-permute-done((bf16[1024,128]{1,0:T(8,128)(2,1)S(1)}, bf16[1024,128]{1,0:T(8,128)(2,1)S(1)}, u32[]{:S(2)}, u32[]{:S(2)}) %collective-permute-start.4) | collective-permute-done | bytes 262176 | tf_op jit(solution)/shard_map/ppermute | solution.py:91
  71.9 12.1 %collective-permute-done.5 = bf16[1024,128]{1,0:T(8,128)(2,1)S(1)} collective-permute-done((bf16[1024,128]{1,0:T(8,128)(2,1)S(1)}, bf16[1024,128]{1,0:T(8,128)(2,1)S(1)}, u32[]{:S(2)}, u32[]{:S(2)}) %collective-permute-start.5) | collective-permute-done | bytes 262176 | tf_op jit(solution)/shard_map/ppermute | solution.py:91
  84.0 18.3 %collective-permute-done.6 = bf16[1024,128]{1,0:T(8,128)(2,1)S(1)} collective-permute-done((bf16[1024,128]{1,0:T(8,128)(2,1)S(1)}, bf16[1024,128]{1,0:T(8,128)(2,1)S(1)}, u32[]{:S(2)}, u32[]{:S(2)}) %collective-permute-start.6) | collective-permute-done | bytes 262176 | tf_op jit(solution)/shard_map/ppermute | solution.py:91
  102.3 15.4 %collective-permute-done.7 = bf16[1024,128]{1,0:T(8,128)(2,1)S(1)} collective-permute-done((bf16[1024,128]{1,0:T(8,128)(2,1)S(1)}, bf16[1024,128]{1,0:T(8,128)(2,1)S(1)}, u32[]{:S(2)}, u32[]{:S(2)}) %collective-permute-start.7) | collective-permute-done | bytes 262176 | tf_op jit(solution)/shard_map/ppermute | solution.py:91
  117.7 10.0 %collective-permute-done.8 = bf16[1024,128]{1,0:T(8,128)(2,1)S(1)} collective-permute-done((bf16[1024,128]{1,0:T(8,128)(2,1)S(1)}, bf16[1024,128]{1,0:T(8,128)(2,1)S(1)}, u32[]{:S(2)}, u32[]{:S(2)}) %collective-permute-start.8) | collective-permute-done | bytes 262176 | tf_op jit(solution)/shard_map/ppermute | solution.py:91
  127.6 10.0 %collective-permute-done.9 = bf16[1024,128]{1,0:T(8,128)(2,1)S(1)} collective-permute-done((bf16[1024,128]{1,0:T(8,128)(2,1)S(1)}, bf16[1024,128]{1,0:T(8,128)(2,1)S(1)}, u32[]{:S(2)}, u32[]{:S(2)}) %collective-permute-start.9) | collective-permute-done | bytes 262176 | tf_op jit(solution)/shard_map/ppermute | solution.py:91
  137.7 9.9 %collective-permute-done.10 = bf16[1024,128]{1,0:T(8,128)(2,1)S(1)} collective-permute-done((bf16[1024,128]{1,0:T(8,128)(2,1)S(1)}, bf16[1024,128]{1,0:T(8,128)(2,1)S(1)}, u32[]{:S(2)}, u32[]{:S(2)}) %collective-permute-start.10) | collective-permute-done | bytes 262176 | tf_op jit(solution)/shard_map/ppermute | solution.py:91
  147.6 17.0 %collective-permute-done.11 = bf16[1024,128]{1,0:T(8,128)(2,1)S(1)} collective-permute-done((bf16[1024,128]{1,0:T(8,128)(2,1)S(1)}, bf16[1024,128]{1,0:T(8,128)(2,1)S(1)}, u32[]{:S(2)}, u32[]{:S(2)}) %collective-permute-start.11) | collective-permute-done | bytes 262176 | tf_op jit(solution)/shard_map/ppermute | solution.py:91
  165.3 12.4 %collective-permute-done.12 = bf16[1024,128]{1,0:T(8,128)(2,1)S(1)} collective-permute-done((bf16[1024,128]{1,0:T(8,128)(2,1)S(1)}, bf16[1024,128]{1,0:T(8,128)(2,1)S(1)}, u32[]{:S(2)}, u32[]{:S(2)}) %collective-permute-start.12) | collective-permute-done | bytes 262176 | tf_op jit(solution)/shard_map/ppermute | solution.py:91
  181.2 8.0 %collective-permute-done.13 = bf16[1024,128]{1,0:T(8,128)(2,1)} collective-permute-done((bf16[1024,128]{1,0:T(8,128)(2,1)S(1)}, bf16[1024,128]{1,0:T(8,128)(2,1)}, u32[]{:S(2)}, u32[]{:S(2)}) %collective-permute-start.13) | collective-permute-done | bytes 262176 | tf_op jit(solution)/shard_map/ppermute | solution.py:91
  191.2 8.3 %collective-permute-done.14 = bf16[1024,128]{1,0:T(8,128)(2,1)} collective-permute-done((bf16[1024,128]{1,0:T(8,128)(2,1)}, bf16[1024,128]{1,0:T(8,128)(2,1)}, u32[]{:S(2)}, u32[]{:S(2)}) %collective-permute-start.14) | collective-permute-done | bytes 262176 | tf_op jit(solution)/shard_map/ppermute | solution.py:91
  227.8 9.6 %fusion.117 = (f32[512]{0:T(512)S(1)}, f32[512]{0:T(512)S(1)}, f32[512,1024]{1,0:T(8,128)}) fusion(bf16[2048,1024]{1,0:T(8,128)(2,1)} %all-gather.11.cloned.1.call-done, bf16[512,2048]{1,0:T(8,128)(2,1)S(1)} %copy-done, f32[2048]{0:T(1024)S(1)} %convert_element_type.144, f32[512]{0:T(512)S(1)} %add_rsqrt_fusion.2), kind=kOutput, calls=%fused_computation.187 | convolution fusion | flops 2186804224 | bytes 8402944 | tf_op jit(solution)/shard_map/dot_general | solution.py:15
  247.1 14.5 %fusion.13 = bf16[512,2048]{1,0:T(8,128)(2,1)} fusion(bf16[1024,4096]{1,0:T(8,128)(2,1)} %constant_dynamic-update-slice_fusion, s32[]{:T(128)S(6)} %select_n.36, f32[64,8,8,128]{3,2,1,0:T(8,128)} %bitcast.50, bf16[2048,1024]{1,0:T(8,128)(2,1)} %all-gather.9.cloned.1.call-done, bf16[512,2048]{1,0:T(8,128)(2,1)S(1)} %copy-done, ...), kind=kOutput, calls=%fused_computation.25 | convolution fusion | flops 4334813184 | bytes 14690308 | tf_op jit(solution)/shard_map/dot_general | solution.py:15
  265.7 13.3 %all-reduce.5.cloned.1.call-done = bf16[512,2048]{1,0:T(8,128)(2,1)} async-done(((bf16[512,2048]{1,0:T(8,128)(2,1)}), bf16[512,2048]{1,0:T(8,128)(2,1)}) %all-reduce.5.cloned.1.call-update) | async-done | bytes 2097168 | tf_op jit(solution)/shard_map/psum | solution.py:96
  282.9 112.2 %all-gather.13.cloned.1.call-done = bf16[2048,2048]{1,0:T(8,128)(2,1)} async-done(((bf16[128,2048]{1,0:T(8,128)(2,1)}), bf16[2048,2048]{1,0:T(8,128)(2,1)}) %all-gather.13.cloned.1.call-update) | async-done | bytes 8388624 | tf_op jit(solution)/shard_map/all_gather | solution.py:101
  395.1 10.1 %convolution_convert_fusion.2 = bf16[512,2048]{1,0:T(8,128)(2,1)} fusion(bf16[2048,2048]{1,0:T(8,128)(2,1)} %all-gather.13.cloned.1.call-done, bf16[512,2048]{1,0:T(8,128)(2,1)} %get-tuple-element.10, f32[2048]{0:T(1024)S(1)} %convert_element_type.155, f32[512]{0:T(512)S(1)} %add_rsqrt_fusion), kind=kOutput, calls=%fused_computation.28 | convolution fusion | flops 4300210176 | bytes 12593152 | tf_op jit(solution)/shard_map/dot_general | solution.py:15
  405.2 103.1 %all-gather.15.cloned.1.call-done = bf16[2048,2048]{1,0:T(8,128)(2,1)} async-done(((bf16[128,2048]{1,0:T(8,128)(2,1)}), bf16[2048,2048]{1,0:T(8,128)(2,1)}) %all-gather.15.cloned.1.call-update) | async-done | bytes 8388624 | tf_op jit(solution)/shard_map/all_gather | solution.py:102
  508.3 8.4 %convolution_convert_fusion.1 = bf16[512,2048]{1,0:T(8,128)(2,1)S(1)} fusion(bf16[2048,2048]{1,0:T(8,128)(2,1)} %all-gather.15.cloned.1.call-done, bf16[512,2048]{1,0:T(8,128)(2,1)S(1)} %copy-done.1, f32[2048]{0:T(1024)S(1)} %convert_element_type.155, f32[512]{0:T(512)S(1)} %add_rsqrt_fusion), kind=kOutput, calls=%fused_computation.27 | convolution fusion | flops 4300210176 | bytes 12593152 | tf_op jit(solution)/shard_map/dot_general | solution.py:15
  522.3 128.7 %all-gather.17.cloned.1.call-done = bf16[2048,2048]{1,0:T(8,128)(2,1)} async-done(((bf16[2048,128]{1,0:T(8,128)(2,1)}), bf16[2048,2048]{1,0:T(8,128)(2,1)}) %all-gather.17.cloned.1.call-update) | async-done | bytes 8388624 | tf_op jit(solution)/shard_map/all_gather | solution.py:109
  651.0 9.9 %convolution_convert_fusion = bf16[512,2048]{1,0:T(8,128)(2,1)} fusion(bf16[512,2048]{1,0:T(8,128)(2,1)} %fusion.7, bf16[2048,2048]{1,0:T(8,128)(2,1)} %all-gather.17.cloned.1.call-done), kind=kOutput, calls=%fused_computation.26 | convolution fusion | flops 4296015872 | bytes 12582912 | tf_op jit(solution)/shard_map/dot_general | solution.py:15
  (115 shorter events, 73.0 us)
Async XLA Ops:
  6.5 182.6 %all-gather.7.cloned.1.call-start = ((), (), s32[]{:S(2)}) async-start(), calls=%async_computation.1 | async-start | bytes 3145728 | tf_op jit(solution)/shard_map/all_gather | solution.py:55
  7.3 220.5 %all-gather.11.cloned.1.call-start = ((), (), s32[]{:S(2)}) async-start(), calls=%async_computation.3 | async-start | bytes 4456448 | tf_op jit(solution)/shard_map/all_gather | solution.py:63
  8.0 239.1 %all-gather.9.cloned.1.call-start = ((), (), s32[]{:S(2)}) async-start(), calls=%async_computation.2 | async-start | bytes 4456448 | tf_op jit(solution)/shard_map/all_gather | solution.py:62
  8.1 13.5 %collective-permute-start = (bf16[1024,128]{1,0:T(8,128)(2,1)}, bf16[1024,128]{1,0:T(8,128)(2,1)S(1)}, u32[]{:S(2)}, u32[]{:S(2)}) collective-permute-start(bf16[1024,128]{1,0:T(8,128)(2,1)} %param.23), channel_id=1, source_target_pairs={{0,2},{2,4},{4,6},{6,8},{8,10},{10,12},{12,14},{14,16},{16,18},{18... | collective-permute-start | bytes 786440 | tf_op jit(solution)/shard_map/ppermute | solution.py:91
  21.6 11.1 %collective-permute-start.1 = (bf16[1024,128]{1,0:T(8,128)(2,1)S(1)}, bf16[1024,128]{1,0:T(8,128)(2,1)S(1)}, u32[]{:S(2)}, u32[]{:S(2)}) collective-permute-start(bf16[1024,128]{1,0:T(8,128)(2,1)S(1)} %collective-permute-done), channel_id=1, source_target_pairs={{0,2},{2,4},{4,6},{6,8},{8,10},{10,12},{12,14},{14,16},{16,18},{18... | collective-permute-start | bytes 786440 | tf_op jit(solution)/shard_map/ppermute | solution.py:91
  32.6 13.3 %collective-permute-start.2 = (bf16[1024,128]{1,0:T(8,128)(2,1)S(1)}, bf16[1024,128]{1,0:T(8,128)(2,1)S(1)}, u32[]{:S(2)}, u32[]{:S(2)}) collective-permute-start(bf16[1024,128]{1,0:T(8,128)(2,1)S(1)} %collective-permute-done.1), channel_id=1, source_target_pairs={{0,2},{2,4},{4,6},{6,8},{8,10},{10,12},{12,14},{14,16},{16,18},{18... | collective-permute-start | bytes 786440 | tf_op jit(solution)/shard_map/ppermute | solution.py:91
  46.0 10.0 %collective-permute-start.3 = (bf16[1024,128]{1,0:T(8,128)(2,1)S(1)}, bf16[1024,128]{1,0:T(8,128)(2,1)S(1)}, u32[]{:S(2)}, u32[]{:S(2)}) collective-permute-start(bf16[1024,128]{1,0:T(8,128)(2,1)S(1)} %collective-permute-done.2), channel_id=1, source_target_pairs={{0,2},{2,4},{4,6},{6,8},{8,10},{10,12},{12,14},{14,16},{16,18},{18... | collective-permute-start | bytes 786440 | tf_op jit(solution)/shard_map/ppermute | solution.py:91
  55.9 16.0 %collective-permute-start.4 = (bf16[1024,128]{1,0:T(8,128)(2,1)S(1)}, bf16[1024,128]{1,0:T(8,128)(2,1)S(1)}, u32[]{:S(2)}, u32[]{:S(2)}) collective-permute-start(bf16[1024,128]{1,0:T(8,128)(2,1)S(1)} %collective-permute-done.3), channel_id=1, source_target_pairs={{0,2},{2,4},{4,6},{6,8},{8,10},{10,12},{12,14},{14,16},{16,18},{18... | collective-permute-start | bytes 786440 | tf_op jit(solution)/shard_map/ppermute | solution.py:91
  71.9 12.1 %collective-permute-start.5 = (bf16[1024,128]{1,0:T(8,128)(2,1)S(1)}, bf16[1024,128]{1,0:T(8,128)(2,1)S(1)}, u32[]{:S(2)}, u32[]{:S(2)}) collective-permute-start(bf16[1024,128]{1,0:T(8,128)(2,1)S(1)} %collective-permute-done.4), channel_id=1, source_target_pairs={{0,2},{2,4},{4,6},{6,8},{8,10},{10,12},{12,14},{14,16},{16,18},{18... | collective-permute-start | bytes 786440 | tf_op jit(solution)/shard_map/ppermute | solution.py:91
  84.0 124.3 %copy-start.4 = (bf16[1024,128]{1,0:T(8,128)(2,1)}, bf16[1024,128]{1,0:T(8,128)(2,1)S(1)}, u32[]{:S(2)}) copy-start(bf16[1024,128]{1,0:T(8,128)(2,1)S(1)} %collective-permute-done.5) | copy-start | bytes 786436
  84.0 18.3 %collective-permute-start.6 = (bf16[1024,128]{1,0:T(8,128)(2,1)S(1)}, bf16[1024,128]{1,0:T(8,128)(2,1)S(1)}, u32[]{:S(2)}, u32[]{:S(2)}) collective-permute-start(bf16[1024,128]{1,0:T(8,128)(2,1)S(1)} %collective-permute-done.5), channel_id=1, source_target_pairs={{0,2},{2,4},{4,6},{6,8},{8,10},{10,12},{12,14},{14,16},{16,18},{18... | collective-permute-start | bytes 786440 | tf_op jit(solution)/shard_map/ppermute | solution.py:91
  102.3 15.4 %collective-permute-start.7 = (bf16[1024,128]{1,0:T(8,128)(2,1)S(1)}, bf16[1024,128]{1,0:T(8,128)(2,1)S(1)}, u32[]{:S(2)}, u32[]{:S(2)}) collective-permute-start(bf16[1024,128]{1,0:T(8,128)(2,1)S(1)} %collective-permute-done.6), channel_id=1, source_target_pairs={{0,2},{2,4},{4,6},{6,8},{8,10},{10,12},{12,14},{14,16},{16,18},{18... | collective-permute-start | bytes 786440 | tf_op jit(solution)/shard_map/ppermute | solution.py:91
  117.7 10.0 %collective-permute-start.8 = (bf16[1024,128]{1,0:T(8,128)(2,1)S(1)}, bf16[1024,128]{1,0:T(8,128)(2,1)S(1)}, u32[]{:S(2)}, u32[]{:S(2)}) collective-permute-start(bf16[1024,128]{1,0:T(8,128)(2,1)S(1)} %collective-permute-done.7), channel_id=1, source_target_pairs={{0,2},{2,4},{4,6},{6,8},{8,10},{10,12},{12,14},{14,16},{16,18},{18... | collective-permute-start | bytes 786440 | tf_op jit(solution)/shard_map/ppermute | solution.py:91
  127.6 10.0 %collective-permute-start.9 = (bf16[1024,128]{1,0:T(8,128)(2,1)S(1)}, bf16[1024,128]{1,0:T(8,128)(2,1)S(1)}, u32[]{:S(2)}, u32[]{:S(2)}) collective-permute-start(bf16[1024,128]{1,0:T(8,128)(2,1)S(1)} %collective-permute-done.8), channel_id=1, source_target_pairs={{0,2},{2,4},{4,6},{6,8},{8,10},{10,12},{12,14},{14,16},{16,18},{18... | collective-permute-start | bytes 786440 | tf_op jit(solution)/shard_map/ppermute | solution.py:91
  137.6 10.0 %collective-permute-start.10 = (bf16[1024,128]{1,0:T(8,128)(2,1)S(1)}, bf16[1024,128]{1,0:T(8,128)(2,1)S(1)}, u32[]{:S(2)}, u32[]{:S(2)}) collective-permute-start(bf16[1024,128]{1,0:T(8,128)(2,1)S(1)} %collective-permute-done.9), channel_id=1, source_target_pairs={{0,2},{2,4},{4,6},{6,8},{8,10},{10,12},{12,14},{14,16},{16,18},{18... | collective-permute-start | bytes 786440 | tf_op jit(solution)/shard_map/ppermute | solution.py:91
  137.6 141.4 %all-reduce.5.cloned.1.call-start = ((), (), s32[]{:S(2)}) async-start(), calls=%async_computation.4 | async-start | bytes 4194304 | tf_op jit(solution)/shard_map/psum | solution.py:96
  147.6 17.0 %collective-permute-start.11 = (bf16[1024,128]{1,0:T(8,128)(2,1)S(1)}, bf16[1024,128]{1,0:T(8,128)(2,1)S(1)}, u32[]{:S(2)}, u32[]{:S(2)}) collective-permute-start(bf16[1024,128]{1,0:T(8,128)(2,1)S(1)} %collective-permute-done.10), channel_id=1, source_target_pairs={{0,2},{2,4},{4,6},{6,8},{8,10},{10,12},{12,14},{14,16},{16,18},{18... | collective-permute-start | bytes 786440 | tf_op jit(solution)/shard_map/ppermute | solution.py:91
  164.6 13.1 %collective-permute-start.12 = (bf16[1024,128]{1,0:T(8,128)(2,1)S(1)}, bf16[1024,128]{1,0:T(8,128)(2,1)S(1)}, u32[]{:S(2)}, u32[]{:S(2)}) collective-permute-start(bf16[1024,128]{1,0:T(8,128)(2,1)S(1)} %collective-permute-done.11), channel_id=1, source_target_pairs={{0,2},{2,4},{4,6},{6,8},{8,10},{10,12},{12,14},{14,16},{16,18},{18... | collective-permute-start | bytes 786440 | tf_op jit(solution)/shard_map/ppermute | solution.py:91
  177.7 11.4 %collective-permute-start.13 = (bf16[1024,128]{1,0:T(8,128)(2,1)S(1)}, bf16[1024,128]{1,0:T(8,128)(2,1)}, u32[]{:S(2)}, u32[]{:S(2)}) collective-permute-start(bf16[1024,128]{1,0:T(8,128)(2,1)S(1)} %collective-permute-done.12), channel_id=1, source_target_pairs={{0,2},{2,4},{4,6},{6,8},{8,10},{10,12},{12,14},{14,16},{16,18},{18... | collective-permute-start | bytes 786440 | tf_op jit(solution)/shard_map/ppermute | solution.py:91
  189.1 10.3 %collective-permute-start.14 = (bf16[1024,128]{1,0:T(8,128)(2,1)}, bf16[1024,128]{1,0:T(8,128)(2,1)}, u32[]{:S(2)}, u32[]{:S(2)}) collective-permute-start(bf16[1024,128]{1,0:T(8,128)(2,1)} %collective-permute-done.13), channel_id=1, source_target_pairs={{0,2},{2,4},{4,6},{6,8},{8,10},{10,12},{12,14},{14,16},{16,18},{18... | collective-permute-start | bytes 786440 | tf_op jit(solution)/shard_map/ppermute | solution.py:91
  261.6 133.5 %all-gather.13.cloned.1.call-start = ((), (), s32[]{:S(2)}) async-start(), calls=%async_computation.5 | async-start | bytes 8912896 | tf_op jit(solution)/shard_map/all_gather | solution.py:101
  262.2 246.0 %all-gather.15.cloned.1.call-start = ((), (), s32[]{:S(2)}) async-start(), calls=%async_computation.6 | async-start | bytes 8912896 | tf_op jit(solution)/shard_map/all_gather | solution.py:102
  262.8 388.2 %all-gather.17.cloned.1.call-start = ((), (), s32[]{:S(2)}) async-start(), calls=%async_computation.7 | async-start | bytes 8912896 | tf_op jit(solution)/shard_map/all_gather | solution.py:109
  263.5 405.3 %reduce-scatter.2.cloned.1.call-start = ((), (), s32[]{:S(2)}) async-start(), calls=%async_computation.8 | async-start | bytes 3145728 | tf_op jit(solution)/shard_map/reduce_scatter | solution.py:113
  (11 other events, 266.6 us)
Sparse Core Ops, SparseCore 0:
  8.9 13.2 all-gather.6
  25.0 93.1 all-gather.10
  137.7 86.9 all-gather.8
  261.7 17.1 all-reduce.4
  281.6 113.4 all-gather.12
  397.8 110.4 all-gather.14
  511.0 139.9 all-gather.16
  661.0 7.7 reduce-scatter.1
